TPU v7x, 32 devices: a whole 2x2x4 slice. The times are simulated.
32 devices in a mesh: ep: 8 (over z, x), tp: 4 (over y, core).
Axes of the slice: x: 2, y: 2, z: 4, core: 2. Of those that a mesh axis runs over, the one named last changes fastest.
Arguments:
- query_in: bfloat16 [4096, 2048], P('ep', 'tp'), may hold values from -6 to 6
- key_in: bfloat16 [4096, 2048], P('ep', 'tp'), may hold values from -6 to 6
- value_in: bfloat16 [4096, 2048], P('ep', 'tp'), may hold values from -6 to 6
- gate_in: bfloat16 [4096, 2048], P('ep', 'tp'), may hold values from -6 to 6
- decay_rate: float32 [16], P('tp'), may hold values from 0 to 0.04
- head_gain: float32 [2048], P('tp'), may hold values from 0.1 to 1.9
- output_weight: bfloat16 [2048, 2048], P('tp'), may hold values from -0.125 to 0.125
- token_rows: bfloat16 [1536, 2048], P('ep'), may hold values from -100 to 100
- token_gain: float32 [2048], replicated, may hold values from 0.1 to 1.9
- route_ids: int32 [1536, 2], P('ep'), may hold values from 0 to 7, all different within a row; in each aligned block of 192 rows (0 to 191, 192 to 383, ...) at most 96 rows name the same one
- route_weights: float32 [1536, 2], P('ep'), may hold values from 0.25 to 2.5
- expert_gate: bfloat16 [8, 2048, 4096], P('ep', None, 'tp'), may hold values from -0.125 to 0.125
- expert_up: bfloat16 [8, 2048, 4096], P('ep', None, 'tp'), may hold values from -0.125 to 0.125
- expert_down: bfloat16 [8, 4096, 2048], P('ep', None, 'tp'), may hold values from -0.09375 to 0.09375
Outputs:
- retained_out: bfloat16 [4096, 2048], P(('ep', 'tp'))
- expert_out: bfloat16 [1536, 2048], P('ep', 'tp')
Inputs may be any that keep to these rules, and one draw needn't show every extreme that they name: `route_ids`: each row names 2 different experts. In each aligned block of 192 rows (the rows of one index of ep) no expert is named by more than 96 rows, a bound that some block reaches.
All inputs are finite; a program needn't handle non-finite values.
Results may differ from a plain program's by a relative error of at most 0.019.
Values may be sent and summed in bfloat16 or wider, within the bound.
A program may use at most 64 MiB of HBM per device.

v0:
```python
import jax
import jax.numpy as jnp
from jax import lax
from jax.sharding import PartitionSpec as P

epsilon = 1e-06
rope_base = 10000.0


def entering(x, axis, combine, identity):
    size, here = (lax.axis_size(axis), lax.axis_index(axis))
    everything = jax.tree.map(lambda part: lax.all_gather(part, axis), x)
    start = jax.tree.map(
        lambda part, zero: jnp.broadcast_to(jnp.asarray(zero, part.dtype), part.shape), x, identity
    )

    def turn(k, before):
        reached = k < here
        new = combine(before, jax.tree.map(lambda part: part[k], everything))
        return jax.tree.map(lambda a, b: jnp.where(reached, a, b), new, before)

    return lax.fori_loop(0, size, turn, start)


def rotate(values, positions):
    half_dim = values.shape[-1] // 2
    frequency = rope_base ** (-jnp.arange(half_dim, dtype=jnp.float32) * 2.0 / values.shape[-1])
    angles = positions.astype(jnp.float32)[:, None] * frequency[None, :]
    cosine_table = jnp.cos(angles)[:, None, :]
    sine_table = jnp.sin(angles)[:, None, :]
    first_half = values[..., :half_dim]
    second = values[..., half_dim:]
    return jnp.concatenate(
        [
            first_half * cosine_table - second * sine_table,
            second * cosine_table + first_half * sine_table,
        ],
        -1,
    )


def retention_part(query_in, key_in, value_in, gate_in, decay_rate, head_gain, output_weight):
    block_len = query_in.shape[0]
    head_count = decay_rate.shape[0]
    key_dim = query_in.shape[1] // head_count
    value_dim = value_in.shape[1] // head_count
    highest = lax.Precision.HIGHEST
    positions = lax.axis_index("ep") * block_len + jnp.arange(block_len, dtype=jnp.int32)
    rot_query = rotate(
        query_in.astype(jnp.float32).reshape(block_len, head_count, key_dim), positions
    ).astype(jnp.bfloat16)
    rot_key = (
        rotate(key_in.astype(jnp.float32).reshape(block_len, head_count, key_dim), positions)
        * key_dim ** (-0.5)
    ).astype(jnp.bfloat16)
    value_heads = value_in.reshape(block_len, head_count, value_dim)
    within = jnp.arange(block_len, dtype=jnp.float32)
    distance = within[:, None] - within[None, :]
    decay_mat = jnp.where(
        distance[None] >= 0,
        jnp.exp(-decay_rate[:, None, None] * jnp.maximum(distance, 0.0)[None]),
        0.0,
    )
    scores = jnp.einsum("ihd,jhd->hij", rot_query, rot_key, preferred_element_type=jnp.float32)
    weights = (scores * decay_mat).astype(jnp.bfloat16)
    local_out = jnp.einsum("hij,jhe->ihe", weights, value_heads, preferred_element_type=jnp.float32)
    key_decay = jnp.exp(-decay_rate[None, :] * (block_len - 1.0 - within)[:, None])
    decayed = (rot_key.astype(jnp.float32) * key_decay[:, :, None]).astype(jnp.bfloat16)
    block_state = jnp.einsum(
        "jhd,jhe->hde", decayed, value_heads, preferred_element_type=jnp.float32
    )
    span_decay = jnp.exp(-decay_rate * block_len)

    def compose(earlier, later):
        return (earlier[0] * later[0], later[0][:, None, None] * earlier[1] + later[1])

    identity = (jnp.ones_like(span_decay), jnp.zeros_like(block_state))
    carried = entering((span_decay, block_state), "ep", compose, identity)[1]
    query_decay = jnp.exp(-decay_rate[None, :] * (within + 1.0)[:, None])
    carried_out = (
        jnp.einsum("ihd,hde->ihe", rot_query.astype(jnp.float32), carried, precision=highest)
        * query_decay[:, :, None]
    )
    retained = local_out + carried_out
    centered = retained - jnp.mean(retained, -1, keepdims=True)
    normed = centered * lax.rsqrt(jnp.mean(centered * centered, -1, keepdims=True) + epsilon)
    mixed = (
        normed.reshape(block_len, head_count * value_dim)
        * head_gain
        * jax.nn.silu(gate_in.astype(jnp.float32))
    ).astype(jnp.bfloat16)
    return lax.psum_scatter(
        jnp.dot(mixed, output_weight, preferred_element_type=jnp.float32).astype(jnp.bfloat16),
        "tp",
        scatter_dimension=0,
        tiled=True,
    )


def finish(gate_pre, up_pre, source_count, slot_count, expert_down):
    hidden = (jax.nn.silu(gate_pre) * up_pre).astype(jnp.bfloat16)
    down_local = expert_down[0]
    result = jnp.dot(
        lax.all_gather(hidden, "tp", axis=1, tiled=True),
        down_local,
        preferred_element_type=jnp.float32,
    ).astype(jnp.bfloat16)
    result = result.reshape(source_count, slot_count, down_local.shape[1])
    return lax.all_to_all(result, "ep", split_axis=0, concat_axis=0, tiled=True)


def expert_part(
    token_rows, token_gain, route_ids, route_weights, expert_gate, expert_up, expert_down
):
    token_count, model_dim = token_rows.shape
    rows_float = token_rows.astype(jnp.float32)
    normed = (
        rows_float
        * lax.rsqrt(jnp.mean(rows_float * rows_float, -1, keepdims=True) + epsilon)
        * token_gain
    ).astype(jnp.bfloat16)
    padded = jnp.concatenate([normed, jnp.zeros((1, model_dim), jnp.bfloat16)], 0)
    expert_count = lax.axis_size("ep")
    top_count = route_ids.shape[1]
    capacity = 2 * token_count * top_count // expert_count
    flat_ids = route_ids.reshape(-1)
    matches = (flat_ids[:, None] == jnp.arange(expert_count, dtype=jnp.int32)[None, :]).astype(
        jnp.int32
    )
    slot_number = jnp.sum((jnp.cumsum(matches, axis=0) - 1) * matches, axis=1)
    slot_index = flat_ids * capacity + slot_number
    token_index = jnp.arange(flat_ids.shape[0], dtype=jnp.int32) // top_count
    slot_table = (
        jnp.full((expert_count * capacity,), token_count, jnp.int32).at[slot_index].set(token_index)
    )
    column_width = model_dim // lax.axis_size("tp")
    column_start = lax.axis_index("tp") * column_width
    own_columns = lax.dynamic_slice_in_dim(padded, column_start, column_width, 1)
    outgoing = own_columns[slot_table].reshape(expert_count, capacity, column_width)
    incoming = lax.all_to_all(outgoing, "ep", split_axis=0, concat_axis=0, tiled=True)
    flat_count = incoming.shape[0] * incoming.shape[1]
    shard_piece = lax.all_gather(incoming, "tp", axis=2, tiled=True)
    piece_rows = shard_piece.reshape(flat_count, shard_piece.shape[2])
    gate_rows = expert_gate[0]
    up_rows = expert_up[0]
    gate_pre = jnp.dot(piece_rows, gate_rows, preferred_element_type=jnp.float32)
    up_pre = jnp.dot(piece_rows, up_rows, preferred_element_type=jnp.float32)
    returned = finish(gate_pre, up_pre, incoming.shape[0], incoming.shape[1], expert_down)
    picked = returned.reshape(expert_count * capacity, returned.shape[2])[slot_index]
    combined = jnp.sum(
        picked.astype(jnp.float32).reshape(token_count, top_count, returned.shape[2])
        * route_weights[:, :, None],
        axis=1,
    )
    return combined.astype(jnp.bfloat16)


def body(
    query_in,
    key_in,
    value_in,
    gate_in,
    decay_rate,
    head_gain,
    output_weight,
    token_rows,
    token_gain,
    route_ids,
    route_weights,
    expert_gate,
    expert_up,
    expert_down,
):
    retained_out = retention_part(
        query_in, key_in, value_in, gate_in, decay_rate, head_gain, output_weight
    )
    expert_out = expert_part(
        token_rows, token_gain, route_ids, route_weights, expert_gate, expert_up, expert_down
    )
    return (retained_out, expert_out)


def solution(mesh):
    placed = (
        P("ep", "tp"),
        P("ep", "tp"),
        P("ep", "tp"),
        P("ep", "tp"),
        P("tp"),
        P("tp"),
        P("tp", None),
        P("ep", None),
        P(),
        P("ep", None),
        P("ep", None),
        P("ep", None, "tp"),
        P("ep", None, "tp"),
        P("ep", None, "tp"),
    )
    return jax.shard_map(
        body,
        mesh=mesh,
        in_specs=placed,
        out_specs=(P(("ep", "tp"), None), P("ep", "tp")),
        check_vma=False,
    )
```

profile of v0, /device:TPU:0, one launch (start us, length us, event | category | flops | bytes accessed | tf_op | source)
XLA Modules:
  0.0 217.2 jit_solution(11615766043707157128)
XLA Ops:
  12.1 2.9 %scatter_custom_fusion = s32[768]{0:T(1024)S(1)} fusion(s32[384]{0:T(512)S(1)} %fusion.43, s32[384]{0:T(512)S(1)} %add_select_fusion, s32[]{:T(128)} %constant.98.clone.1), kind=kCustom, calls=%fused_computation.78 | custom fusion | bytes 3076 | tf_op jit(solution)/shard_map/scatter | solution.py:134
  15.0 1.4 fusion.11
  16.4 2.7 %gather_fusion = bf16[768,512]{1,0:T(8,128)(2,1)S(1)} fusion(bf16[193,512]{1,0:T(8,128)(2,1)S(1)} %pad_dynamic-slice_fusion, s32[1024]{0:T(1024)S(1)} %pad_clamp_fusion.1), kind=kCustom, calls=%fused_computation | custom fusion | bytes 1575936 | tf_op jit(solution)/shard_map/gather | solution.py:139
  19.1 27.3 %all_to_all.10 = bf16[8,96,512]{2,1,0:T(8,128)(2,1)} all-to-all(bf16[8,96,512]{2,1,0:T(8,128)(2,1)S(1)} %bitcast.71), channel_id=1, replica_groups=mesh['ep'=8,'tp'=4] {'ep'}, dimensions={0} | all-to-all | bytes 1572864 | tf_op jit(solution)/shard_map/all_to_all | solution.py:140
  48.7 2.4 %copy.54 = f32[512,4,64]{2,0,1:T(8,128)} copy(f32[512,4,64]{0,2,1:T(8,128)} %get-tuple-element.132) | data formatting | bytes 1048576
  54.8 2.5 %copy.56 = f32[512,4,64]{2,0,1:T(8,128)} copy(f32[512,4,64]{0,2,1:T(8,128)} %get-tuple-element.134) | data formatting | bytes 1048576
  57.3 2.4 %copy.57 = f32[512,4,64]{2,0,1:T(8,128)} copy(f32[512,4,64]{0,2,1:T(8,128)} %get-tuple-element.133) | data formatting | bytes 1048576
  62.0 3.5 %subtract_convert_fusion = (bf16[512,4,64]{2,0,1:T(8,128)(2,1)}, bf16[512,4,64]{2,0,1:T(8,128)(2,1)}, f32[512,4,64]{2,0,1:T(8,128)S(1)}, f32[512,4,64]{2,0,1:T(8,128)S(1)}) fusion(f32[512,4,64]{2,0,1:T(8,128)} %copy.55, f32[512,4,64]{2,0,1:T(8,128)S(1)} %copy-done.1, f32[512,64]{1,0:T(8,128)S(1)} %get-tuple-element.136, ...), kind=kLoop, calls=%fused_computation.42 | loop fusion | flops 1835008 | bytes 3932160 | tf_op jit(solution)/shard_map/convert.3
  66.6 1.5 fusion.28
  68.2 6.0 %all-gather.6.cloned.1.call-done = bf16[8,96,2048]{2,1,0:T(8,128)(2,1)} async-done(((bf16[8,96,512]{2,1,0:T(8,128)(2,1)}), bf16[8,96,2048]{2,1,0:T(8,128)(2,1)}) %all-gather.6.cloned.1.call-update) | async-done | bytes 3145744 | tf_op jit(solution)/shard_map/all_gather | solution.py:142
  74.2 6.3 %fusion.3 = f32[768,1024]{1,0:T(8,128)S(1)} fusion(bf16[768,2048]{1,0:T(8,128)(2,1)} %bitcast.75, bf16[1,2048,1024]{2,1,0:T(8,128)(2,1)} %param.28), kind=kOutput, calls=%fused_computation.8 | convolution fusion | flops 3221225472 | bytes 10485760 | tf_op jit(solution)/shard_map/dot_general | solution.py:147
  80.5 5.0 %multiply_convert_fusion.1 = bf16[768,1024]{1,0:T(8,128)(2,1)} fusion(f32[768,1024]{1,0:T(8,128)S(1)} %fusion.3, bf16[768,2048]{1,0:T(8,128)(2,1)S(1)} %bitcast.76, bf16[1,2048,1024]{2,1,0:T(8,128)(2,1)S(1)} %copy-done.7), kind=kOutput, calls=%fused_computation.13 | convolution fusion | flops 3225944064 | bytes 12058624 | tf_op jit(solution)/shard_map/dot_general | solution.py:146
  85.6 21.8 %all-reduce.1 = f32[32]{0:T(128)S(1)} all-reduce(f32[32]{0:T(128)S(1)} %get-tuple-element.139), channel_id=2, replica_groups=mesh['ep'=8,'tp'=4] {'ep'}, use_global_device_ids=true, to_apply=%add.1 | all-reduce | flops 32 | bytes 256
  109.6 4.6 %fusion.16 = f32[512,4,128]{0,2,1:T(8,128)} fusion(bf16[512,4,128]{2,0,1:T(8,128)(2,1)} %copy-done.4, f32[512,512]{1,0:T(8,128)} %fusion.24, f32[4]{0:T(128)S(1)} %get-tuple-element.140, pred[512,512]{1,0:T(8,128)(4,1)} %fusion.25, bf16[512,4,64]{2,0,1:T(8,128)(2,1)S(1)} %copy-done.3, bf16[512,4,64]{2,0,1:T(8,128)(2,1)S(1)} %copy-done.2, ...), kind=kOutput, calls=%fused_computation.22 | convolution fusion | flops 542113792 | bytes 3932176 | tf_op jit(solution)/shard_map/hij,jhe->ihe/dot_general | solution.py:66
  114.2 11.3 %all-gather.10.cloned.1.call-done = f32[32,128,128]{2,1,0:T(8,128)} async-done(((f32[4,128,128]{2,1,0:T(8,128)}), f32[32,128,128]{2,1,0:T(8,128)}) %all-gather.10.cloned.1.call-update) | async-done | bytes 2097168 | tf_op jit(solution)/shard_map/all_gather | solution.py:12
  125.5 8.8 %while.14 = (s32[]{:T(128)}, f32[4,128,128]{2,1,0:T(8,128)S(1)}, s32[]{:T(128)}, f32[8,4]{1,0:T(8,128)S(1)}, f32[8,4,128,128]{3,2,1,0:T(8,128)}, /*index=5*/s32[]{:T(128)}, s32[]{:T(128)}) while((s32[]{:T(128)}, f32[4,128,128]{2,1,0:T(8,128)S(1)}, s32[]{:T(128)}, f32[8,4]{1,0:T(8,128)S(1)}, f32[8,4,128,128]{3,2,1,0:T(8,128)}, ...), condition=%wide.region_1.2_spmd.clone, body=%wide.region_0.1_spmd.clone.sunk | while | flops 262148 | bytes 786585 | solution.py:22
  134.3 2.1 fusion.51
  138.1 4.1 %convolution_convert_fusion = bf16[512,2048]{1,0:T(8,128)(2,1)} fusion(bf16[512,2048]{1,0:T(8,128)(2,1)S(1)} %copy-done, bf16[512,512]{1,0:T(8,128)(2,1)} %param.19, f32[512,512]{1,0:T(8,128)} %copy.47, f32[512]{0:T(512)S(1)} %copy-done.10), kind=kOutput, calls=%fused_computation.14 | convolution fusion | flops 1076887552 | bytes 5769216 | tf_op jit(solution)/shard_map/dot_general | solution.py:93
  142.2 29.7 %all-gather.8.cloned.1.call-done = bf16[768,4096]{1,0:T(8,128)(2,1)} async-done(((bf16[768,1024]{1,0:T(8,128)(2,1)}), bf16[768,4096]{1,0:T(8,128)(2,1)}) %all-gather.8.cloned.1.call-update) | async-done | bytes 6291472 | tf_op jit(solution)/shard_map/all_gather | solution.py:104
  172.0 8.3 %fusion.13 = bf16[768,512]{1,0:T(8,128)(2,1)} fusion(bf16[768,4096]{1,0:T(8,128)(2,1)} %all-gather.8.cloned.1.call-done, bf16[1,4096,512]{2,1,0:T(8,128)(2,1)} %param.29), kind=kOutput, calls=%fused_computation.21 | convolution fusion | flops 3221618688 | bytes 11272192 | tf_op jit(solution)/shard_map/dot_general | solution.py:103
  180.3 5.5 %all-to-all-start.1 = ((bf16[8,96,512]{2,1,0:T(8,128)(2,1)}), bf16[8,96,512]{2,1,0:T(8,128)(2,1)S(1)}, u32[]{:S(2)}, u32[]{:S(2)}) async-start(bf16[8,96,512]{2,1,0:T(8,128)(2,1)} %bitcast.73), calls=%async_computation.2 | async-start | bytes 1572864 | tf_op jit(solution)/shard_map/all_to_all | solution.py:109
  186.0 20.4 %all-to-all-done.1 = bf16[8,96,512]{2,1,0:T(8,128)(2,1)S(1)} async-done(((bf16[8,96,512]{2,1,0:T(8,128)(2,1)}), bf16[8,96,512]{2,1,0:T(8,128)(2,1)S(1)}, u32[]{:S(2)}, u32[]{:S(2)}) %all-to-all-start.1) | async-done | bytes 786464 | tf_op jit(solution)/shard_map/all_to_all | solution.py:109
  206.4 2.1 gather_fusion.1
  209.0 1.7 multiply_reduce_fusion.1
  (93 shorter events, 26.9 us)
Async XLA Ops:
  7.2 131.0 %copy-start = (bf16[512,2048]{1,0:T(8,128)(2,1)S(1)}, bf16[512,2048]{1,0:T(8,128)(2,1)}, u32[]{:S(2)}) copy-start(bf16[512,2048]{1,0:T(8,128)(2,1)} %param.22) | copy-start | bytes 6291460
  7.2 67.0 %all-gather.6.cloned.1.call-start = ((), (), s32[]{:S(2)}) async-start(), calls=%async_computation.4 | async-start | bytes 3932160 | tf_op jit(solution)/shard_map/all_gather | solution.py:142
  46.5 79.0 %all-gather.10.cloned.1.call-start = ((), (), s32[]{:S(2)}) async-start(), calls=%async_computation.6 | async-start | bytes 2359296 | tf_op jit(solution)/shard_map/all_gather | solution.py:12
  52.4 7.3 %copy-start.11 = (u32[32]{0:T(128)S(1)}, u32[32]{0:T(128)}, u32[]{:S(2)}) copy-start(u32[32]{0:T(128)} %constant.111) | copy-start | bytes 388
  54.8 7.1 %copy-start.1 = (f32[512,4,64]{2,0,1:T(8,128)S(1)}, f32[512,4,64]{2,0,1:T(8,128)}, u32[]{:S(2)}) copy-start(f32[512,4,64]{2,0,1:T(8,128)} %copy.54) | copy-start | bytes 1572868
  62.0 3.9 %copy-start.6 = (f32[4]{0:T(128)S(1)}, f32[4]{0:T(128)}, u32[]{:S(2)}) copy-start(f32[4]{0:T(128)} %param.20) | copy-start | bytes 52
  62.0 4.6 %copy-start.9 = (bf16[512,512]{1,0:T(8,128)(2,1)S(1)}, bf16[512,512]{1,0:T(8,128)(2,1)}, u32[]{:S(2)}) copy-start(bf16[512,512]{1,0:T(8,128)(2,1)} %param.18) | copy-start | bytes 1572868
  65.8 0.8 copy-start.4
  68.1 103.8 %all-gather.8.cloned.1.call-start = ((), (), s32[]{:S(2)}) async-start(), calls=%async_computation.5 | async-start | bytes 7864320 | tf_op jit(solution)/shard_map/all_gather | solution.py:104
  74.2 6.3 %copy-start.7 = (bf16[1,2048,1024]{2,1,0:T(8,128)(2,1)S(1)}, bf16[1,2048,1024]{2,1,0:T(8,128)(2,1)}, u32[]{:S(2)}) copy-start(bf16[1,2048,1024]{2,1,0:T(8,128)(2,1)} %param.27) | copy-start | bytes 12582916
  74.2 6.3 %copy-start.8 = (bf16[8,96,2048]{2,1,0:T(8,128)(2,1)S(1)}, bf16[8,96,2048]{2,1,0:T(8,128)(2,1)}, u32[]{:S(2)}) copy-start(bf16[8,96,2048]{2,1,0:T(8,128)(2,1)} %all-gather.6.cloned.1.call-done) | copy-start | bytes 9437188
  80.5 29.1 %copy-start.2 = (bf16[512,4,64]{2,0,1:T(8,128)(2,1)S(1)}, bf16[512,4,64]{2,0,1:T(8,128)(2,1)}, u32[]{:S(2)}) copy-start(bf16[512,4,64]{2,0,1:T(8,128)(2,1)} %get-tuple-element.125) | copy-start | bytes 786436
  80.5 29.1 %copy-start.3 = (bf16[512,4,64]{2,0,1:T(8,128)(2,1)S(1)}, bf16[512,4,64]{2,0,1:T(8,128)(2,1)}, u32[]{:S(2)}) copy-start(bf16[512,4,64]{2,0,1:T(8,128)(2,1)} %get-tuple-element.126) | copy-start | bytes 786436
  85.5 125.1 %reduce-scatter.2.cloned.1.call-start = ((), (), s32[]{:S(2)}) async-start(), calls=%async_computation.3 | async-start | bytes 2621440 | tf_op jit(solution)/shard_map/reduce_scatter | solution.py:92
  136.4 1.7 copy-start.10
  142.2 43.6 %copy-start.5 = (f32[192,2]{0,1:T(2,128)S(1)}, f32[192,2]{0,1:T(2,128)}, u32[]{:S(2)}) copy-start(f32[192,2]{0,1:T(2,128)} %param.26) | copy-start | bytes 4612
  180.3 26.1 %all-to-all-start.1 = ((bf16[8,96,512]{2,1,0:T(8,128)(2,1)}), bf16[8,96,512]{2,1,0:T(8,128)(2,1)S(1)}, u32[]{:S(2)}, u32[]{:S(2)}) async-start(bf16[8,96,512]{2,1,0:T(8,128)(2,1)} %bitcast.73), calls=%async_computation.2 | async-start | bytes 1572864 | tf_op jit(solution)/shard_map/all_to_all | solution.py:109
Sparse Core Ops, SparseCore 0:
  46.6 27.5 all-gather.5
  76.3 49.1 all-gather.9
  127.0 44.8 all-gather.7
  174.9 31.1 reduce-scatter.1
where the time goes:
time: 218 us; the launch traced here: 217 us
  waiting for transfers between devices  67.5 us (31%)
  blocking collectives  49.1 us (23%)
  matrix products  31.9 us (15%)
  local copies, waits for them, and re-layouts  25.9 us (12%)
  other arithmetic  22.2 us (10%)
  between operations  14.8 us (7%)
  starting transfers between devices  5.67 us (3%)
    all_gather x1, waiting for transfers between devices, finish(): lax.all_gather(hidden, 'tp', axis=1, tiled=True)  29.7 us
    all_to_all x1, blocking collectives, expert_part(): lax.all_to_all(outgoing, 'ep', split_axis=0, concat_axis=0, tiled=True)  27.3 us
    unnamed x1, blocking collectives  21.8 us
    all_to_all x1, waiting for transfers between devices, finish(): return lax.all_to_all(result, 'ep', split_axis=0, concat_axis=0, tiled=True)  20.4 us
    unnamed x34, local copies, waits for them, and re-layouts  13.4 us
    all_gather x1, waiting for transfers between devices, entering(): everything = jax.tree.map(lambda part: lax.all_gather(part, axis), x)  11.3 us
    select_n x8, other arithmetic, turn(): return jax.tree.map(lambda a, b: jnp.where(reached, a, b), new, before)  8.52 us
    dot_general x1, matrix products, finish(): jnp.dot(lax.all_gather(hidden, 'tp', axis=1, tiled=True), down_local, pre...  8.35 us
  transfers between devices with their start and end apart: 5, of which 4 were waited for; matrix products, arithmetic and copies ran while one was open for 31% of the time, Pallas kernels for 0%

commit v1 on v0

v1 whole, which is shorter than its diff:
```python
import functools

import jax
import jax.numpy as jnp
from jax import lax
from jax.experimental import pallas as pl
from jax.experimental.pallas import tpu as pltpu
from jax.sharding import PartitionSpec as P

epsilon = 1e-06
rope_base = 10000.0
F32 = jnp.float32
BF16 = jnp.bfloat16
MESH = pl.DeviceIdType.MESH


def dot(a, b):
    return jnp.dot(a, b, preferred_element_type=F32)


def iota(shape, dim):
    return lax.broadcasted_iota(jnp.int32, shape, dim)


def silu(v):
    return v / (1.0 + jnp.exp(-v))


def kernel(
    size,
    tok, tgain, ids, ids_t, rweights, decay, hgain, cos_t, sin_t,
    query_h, key_h, value_h, gate_h, ow_h, wg_h, wu_h, wd_h,
    ret_out, exp_out,
    query, key, value, gate, ow, wg, wu, wd,
    obuf, xbuf, hbuf, sbuf, rbuf, w_hi, w_lo,
    rq, rk, local, state, st_send, st_recv, mixed, part, rs1, rs2_send, rs2_recv,
    load_sem, d_send, d_recv, xy_send, xy_recv, xc_send, xc_recv,
    hy_send, hy_recv, hc_send, hc_recv, b_send, b_recv, st_ssem, st_rsem,
    r1_send, r1_recv, r2_send, r2_recv,
):
    ep, tp, cap, fan, rounds, nf, nm = (
        size["ep"], size["tp"], size["cap"], size["fan"], size["rounds"], size["nf"], size["nm"]
    )
    ys = tp // 2
    e, t = lax.axis_index("ep"), lax.axis_index("tp")
    y, c = t // 2, lax.rem(t, 2)
    mate = (e, y * 2 + 1 - c)
    heads = decay.shape[0]
    tokens, model = tok.shape
    cw = model // tp
    block_len = query.shape[0]
    dk = query.shape[1] // heads

    def over_ep(offset):
        return (lax.rem(e + offset, ep), t)

    def y_at(offset):
        return lax.rem(y + offset, ys)

    def over_y(offset):
        return (e, y_at(offset) * 2 + c)

    def remote(src, dst, ssem, rsem, device):
        return pltpu.make_async_remote_copy(
            src_ref=src, dst_ref=dst, send_sem=ssem, recv_sem=rsem,
            device_id=device, device_id_type=MESH,
        )

    sent = []

    def send(src, dst, ssem, rsem, device):
        copy = remote(src, dst, ssem, rsem, device)
        copy.start()
        sent.append(copy)

    def arrived(dst, ssem, rsem, device):
        remote(dst, dst, ssem, rsem, device).wait_recv()

    loads = [
        pltpu.make_async_copy(a, b, load_sem.at[i])
        for i, (a, b) in enumerate(
            ((query_h, query), (key_h, key), (value_h, value), (gate_h, gate),
             (wg_h, wg), (wu_h, wu), (ow_h, ow), (wd_h, wd))
        )
    ]
    for copy in loads:
        copy.start()

    barrier = pltpu.get_barrier_semaphore()
    friends = [over_ep(i) for i in range(1, ep)] + [over_y(i) for i in range(1, ys)] + [mate]
    for friend in friends:
        pl.semaphore_signal(barrier, inc=1, device_id=friend, device_id_type=MESH)

    def relative(v):
        return jnp.where(v < e, v - e + ep, v - e)

    rel = relative(ids[...])
    rel_t = relative(ids_t[...])
    lanes = max(ep, 128)
    named0 = iota((tokens, lanes), 1) == rel[:, 0:1]
    named1 = iota((tokens, lanes), 1) == rel[:, 1:2]
    named = jnp.where(named0 | named1, 1.0, 0.0)
    before = jnp.where(iota((tokens, tokens), 1) < iota((tokens, tokens), 0), 1.0, 0.0)
    rank = dot(before.astype(BF16), named.astype(BF16))
    pos0 = rel[:, 0:1] * cap + jnp.sum(
        jnp.where(named0, rank, 0.0), 1, keepdims=True).astype(jnp.int32)
    pos1 = rel[:, 1:2] * cap + jnp.sum(
        jnp.where(named1, rank, 0.0), 1, keepdims=True).astype(jnp.int32)
    rows = max(ep, 16)
    named0_t = iota((rows, tokens), 0) == rel_t[0:1, :]
    named1_t = iota((rows, tokens), 0) == rel_t[1:2, :]
    named_t = jnp.where(named0_t | named1_t, 1.0, 0.0)
    after = jnp.where(iota((tokens, tokens), 0) < iota((tokens, tokens), 1), 1.0, 0.0)
    rank_t = dot(named_t.astype(BF16), after.astype(BF16))
    pos0_t = rel_t[0:1, :] * cap + jnp.sum(
        jnp.where(named0_t, rank_t, 0.0), 0, keepdims=True).astype(jnp.int32)
    pos1_t = rel_t[1:2, :] * cap + jnp.sum(
        jnp.where(named1_t, rank_t, 0.0), 0, keepdims=True).astype(jnp.int32)

    rows_float = tok[...].astype(F32)
    scale = lax.rsqrt(jnp.mean(rows_float * rows_float, -1, keepdims=True) + epsilon)
    own = pl.ds(pl.multiple_of(t * cw, cw), cw)
    normed = (tok[:, own].astype(F32) * scale * tgain[:, own]).astype(BF16)
    row_id = iota((ep * cap, tokens), 0)
    pick = jnp.where((row_id == pos0_t) | (row_id == pos1_t), 1.0, 0.0).astype(BF16)
    obuf[...] = dot(pick, normed).astype(BF16)

    pl.semaphore_wait(barrier, len(friends))

    def block(j, n=1):
        return pl.ds(j * cap, n * cap)

    for j in range(ep - 1, 0, -1):
        back = ep - j
        send(obuf.at[block(j)], xbuf.at[t, block(back)], d_send.at[j], d_recv.at[back], over_ep(j))
    xbuf[t, block(0), :] = obuf[block(0), :]

    for copy in loads[:3]:
        copy.wait()
    within = iota((block_len, 1), 0).astype(F32)

    def head_cols(h):
        return pl.ds(pl.multiple_of(h * dk, dk), dk)

    def turn(x):
        return x * cos_t[...] + pltpu.roll(x, dk // 2, 1) * sin_t[...]

    def head_state(h, carry):
        cols = head_cols(h)
        rate = decay[h]
        rq[:, cols] = turn(query[:, cols].astype(F32)).astype(BF16)
        rot_key = (turn(key[:, cols].astype(F32)) * dk ** (-0.5)).astype(BF16)
        rk[:, cols] = rot_key
        decayed = (rot_key.astype(F32) * jnp.exp(-rate * (block_len - 1.0 - within))).astype(BF16)
        now = lax.dot_general(
            decayed, value[:, cols], (((0,), (0,)), ((), ())), preferred_element_type=F32)
        st_send[0, h] = now.astype(BF16)
        return carry

    lax.fori_loop(0, heads, head_state, 0)
    for i in range(1, fan + 1):
        send(st_send.at[0], st_recv.at[i - 1], st_ssem.at[i - 1], st_rsem.at[i - 1], over_ep(i))

    col = iota((tokens, ep * cap), 1)
    weight = jnp.where(col == pos0, rweights[:, 0:1], 0.0) + jnp.where(
        col == pos1, rweights[:, 1:2], 0.0)
    high = weight.astype(BF16)
    w_hi[...] = high
    w_lo[...] = (weight - high.astype(F32)).astype(BF16)

    chunk = min(128, block_len)

    def head_local(h):
        cols = head_cols(h)
        rate = decay[h]
        key_grow = jnp.exp(rate * iota((1, block_len), 1).astype(F32))

        def step(i, carry):
            rws = pl.ds(pl.multiple_of(i * chunk, chunk), chunk)
            place = i * chunk + iota((chunk, 1), 0)
            scores = lax.dot_general(
                rq[rws, cols], rk[:, cols], (((1,), (1,)), ((), ())), preferred_element_type=F32)
            fade = jnp.exp(-rate * place.astype(F32)) * key_grow
            seen = iota((chunk, block_len), 1) <= place
            weights = jnp.where(seen, scores * fade, 0.0).astype(BF16)
            local[rws, cols] = dot(weights, value[:, cols])
            return carry

        lax.fori_loop(0, block_len // chunk, step, 0)

    def spread(buf, piece, rws, ysend, yrecv, csend, crecv, g):
        for a in range(1, ys):
            send(buf.at[piece, rws], buf.at[piece, rws], ysend.at[a, g], yrecv.at[a, g], over_y(a))
        send(buf.at[piece, rws], buf.at[piece, rws], csend.at[0, g], crecv.at[0, g], mate)

    def pass_on(buf, rws, ysend, yrecv, csend, crecv, g):
        for a in range(1, ys):
            piece = y_at(ys - a) * 2 + c
            arrived(buf.at[piece, rws], ysend.at[a, g], yrecv.at[a, g], over_y(a))
            send(buf.at[piece, rws], buf.at[piece, rws], csend.at[a, g], crecv.at[a, g], mate)

    def collect(buf, rws, csend, crecv, g):
        for a in range(ys):
            piece = y_at(ys - a) * 2 + 1 - c
            arrived(buf.at[piece, rws], csend.at[a, g], crecv.at[a, g], mate)

    per_f = ep // nf
    done = 0
    for f in range(nf):
        for k in range(f * per_f, (f + 1) * per_f):
            if k > 0:
                arrived(xbuf.at[t, block(k)], d_send.at[k], d_recv.at[k], over_ep(k))
        spread(xbuf, t, block(f * per_f, per_f), xy_send, xy_recv, xc_send, xc_recv, f)
        if f > 0:
            pass_on(xbuf, block((f - 1) * per_f, per_f), xy_send, xy_recv, xc_send, xc_recv, f - 1)
        upto = heads * (f + 1) // nf
        for h in range(done, upto):
            head_local(h)
        done = upto
    last = nf - 1
    f_per_m = nf // nm
    per_m = ep // nm
    ff = wg.shape[1]
    n_tile = min(256, ff)
    loads[4].wait()
    loads[5].wait()

    def lane(h, times):
        return jnp.exp(jnp.full((1, dk), -decay[h] * (block_len * times), F32))

    def first_state():
        for i in range(fan):
            arrived(st_recv.at[i], st_ssem.at[i], st_rsem.at[i], over_ep(i + 1))

        def one(h, carry):
            total = jnp.zeros((dk, dk), F32)
            for i in range(fan):
                took = st_recv[i, h].astype(F32) * lane(h, float(i))
                total += jnp.where(e > i, took, 0.0)
            state[h] = total
            return carry

        lax.fori_loop(0, heads, one, 0)

    def state_send(r):
        def one(h, carry):
            st_send[r + 1, h] = state[h].astype(BF16)
            return carry

        lax.fori_loop(0, heads, one, 0)
        send(st_send.at[r + 1], st_recv.at[fan + r], st_ssem.at[fan + r], st_rsem.at[fan + r],
             over_ep(fan * 2**r))

    def state_take(r):
        offset = fan * 2**r
        arrived(st_recv.at[fan + r], st_ssem.at[fan + r], st_rsem.at[fan + r], over_ep(offset))

        def one(h, carry):
            took = st_recv[fan + r, h].astype(F32) * lane(h, float(offset))
            state[h] = state[h] + jnp.where(e >= offset, took, 0.0)
            return carry

        lax.fori_loop(0, heads, one, 0)

    for m in range(nm):
        for f in range(m * f_per_m, (m + 1) * f_per_m):
            if f == last:
                pass_on(xbuf, block(f * per_f, per_f), xy_send, xy_recv, xc_send, xc_recv, f)
            collect(xbuf, block(f * per_f, per_f), xc_send, xc_recv, f)
        rws = block(m * per_m, per_m)

        def tile(n, carry):
            cols = pl.ds(pl.multiple_of(n * n_tile, n_tile), n_tile)
            g = u = None
            for p in range(tp):
                x = xbuf[p, rws, :]
                ins = pl.ds(p * cw, cw)
                gp, up = dot(x, wg[ins, cols]), dot(x, wu[ins, cols])
                g, u = (gp, up) if g is None else (g + gp, u + up)
            hbuf[t, rws, cols] = (silu(g) * u).astype(BF16)
            return carry

        lax.fori_loop(0, ff // n_tile, tile, 0)
        spread(hbuf, t, rws, hy_send, hy_recv, hc_send, hc_recv, m)
        if m == 0:
            first_state()
            if rounds:
                state_send(0)
    for r in range(rounds):
        if r > 0:
            state_send(r)
        state_take(r)

    loads[3].wait()
    loads[6].wait()

    def finish(n, carry):
        h, i = n // (block_len // chunk), lax.rem(n, block_len // chunk)
        cols = head_cols(h)
        rws = pl.ds(pl.multiple_of(i * chunk, chunk), chunk)
        place = (i * chunk + iota((chunk, 1), 0)).astype(F32)
        held = state[h]
        high = held.astype(BF16)
        low = (held - high.astype(F32)).astype(BF16)
        q = rq[rws, cols]
        retained = local[rws, cols] + (dot(q, high) + dot(q, low)) * jnp.exp(
            -decay[h] * (place + 1.0))
        centered = retained - jnp.mean(retained, -1, keepdims=True)
        out = centered * lax.rsqrt(jnp.mean(centered * centered, -1, keepdims=True) + epsilon)
        mixed[rws, cols] = (out * hgain[:, cols] * silu(gate[rws, cols].astype(F32))).astype(BF16)
        return carry

    lax.fori_loop(0, heads * (block_len // chunk), finish, 0)
    rb = block_len // tp
    o_tile = min(512, model)

    def project(n, carry):
        cols = pl.ds(pl.multiple_of(n * o_tile, o_tile), o_tile)
        for d in range(tp):
            part[d, :, cols] = dot(mixed[pl.ds(d * rb, rb), :], ow[:, cols]).astype(BF16)
        return carry

    lax.fori_loop(0, model // o_tile, project, 0)
    for b in range(ys):
        send(part.at[b * 2 + 1 - c], rs1.at[b], r1_send.at[b], r1_recv.at[b], mate)

    def h_pass(m):
        pass_on(hbuf, block(m * per_m, per_m), hy_send, hy_recv, hc_send, hc_recv, m)

    def sum_over_cores():
        for b in range(ys):
            arrived(rs1.at[b], r1_send.at[b], r1_recv.at[b], mate)
        for a in range(1, ys):
            b = y_at(a)
            rs2_send[a - 1] = (part[b * 2 + c].astype(F32) + rs1[b].astype(F32)).astype(BF16)
            send(rs2_send.at[a - 1], rs2_recv.at[a - 1], r2_send.at[a - 1], r2_recv.at[a - 1],
                 over_y(a))

    d_tile = min(256, cw)
    loads[7].wait()
    for m in range(nm):
        h_pass(m)
        if m == 0:
            sum_over_cores()
        rws = block(m * per_m, per_m)
        collect(hbuf, rws, hc_send, hc_recv, m)

        def down(n, carry):
            cols = pl.ds(pl.multiple_of(n * d_tile, d_tile), d_tile)
            total = None
            for p in range(tp):
                now = dot(hbuf[p, rws, :], wd[pl.ds(p * ff, ff), cols])
                total = now if total is None else total + now
            sbuf[rws, cols] = total.astype(BF16)
            return carry

        lax.fori_loop(0, cw // d_tile, down, 0)
        for k in range(m * per_m, (m + 1) * per_m):
            if k > 0:
                back = ep - k
                send(sbuf.at[block(k)], rbuf.at[block(back)], b_send.at[k], b_recv.at[back],
                     over_ep(k))
            else:
                rbuf[block(0), :] = sbuf[block(0), :]

    total = part[t].astype(F32) + rs1[y].astype(F32)
    for a in range(1, ys):
        arrived(rs2_recv.at[a - 1], r2_send.at[a - 1], r2_recv.at[a - 1], over_y(a))
        total += rs2_recv[a - 1].astype(F32)
    ret_out[...] = total.astype(BF16)
    for k in range(1, ep):
        arrived(rbuf.at[block(k)], b_send.at[k], b_recv.at[k], over_ep(k))
    exp_out[...] = (dot(w_hi[...], rbuf[...]) + dot(w_lo[...], rbuf[...])).astype(BF16)
    for copy in sent:
        copy.wait_send()


def body(
    query_in, key_in, value_in, gate_in, decay_rate, head_gain, output_weight,
    token_rows, token_gain, route_ids, route_weights, expert_gate, expert_up, expert_down,
):
    ep, tp = lax.axis_size("ep"), lax.axis_size("tp")
    tokens, model = token_rows.shape
    top = route_ids.shape[1]
    cap = -(-(2 * tokens * top // ep) // 32) * 32
    block_len, width = query_in.shape
    heads = decay_rate.shape[0]
    dk = width // heads
    ff = expert_gate.shape[2]
    cw = expert_down.shape[2]
    ys = tp // 2
    fan = min(4, ep - 1)
    rounds = 0
    while fan * 2**rounds < ep - 1:
        rounds += 1
    nf, nm = 4, 2
    half = dk // 2
    positions = lax.axis_index("ep") * block_len + jnp.arange(block_len, dtype=jnp.int32)
    frequency = rope_base ** (-jnp.arange(half, dtype=F32) * 2.0 / dk)
    angles = positions.astype(F32)[:, None] * frequency[None, :]
    cosine, sine = jnp.cos(angles), jnp.sin(angles)
    cos_t = jnp.concatenate([cosine, cosine], -1)
    sin_t = jnp.concatenate([-sine, sine], -1)
    size = dict(ep=ep, tp=tp, cap=cap, fan=fan, rounds=rounds, nf=nf, nm=nm)
    slots = ep * cap
    rb = block_len // tp
    vmem = pl.BlockSpec(memory_space=pltpu.VMEM)
    smem = pl.BlockSpec(memory_space=pltpu.SMEM)
    hbm = pl.BlockSpec(memory_space=pl.ANY)
    dma = pltpu.SemaphoreType.DMA
    big = [query_in, key_in, value_in, gate_in, output_weight,
           expert_gate[0], expert_up[0], expert_down[0]]
    held = big
    return pl.pallas_call(
        functools.partial(kernel, size),
        out_shape=(
            jax.ShapeDtypeStruct((rb, model), BF16),
            jax.ShapeDtypeStruct((tokens, cw), BF16),
        ),
        in_specs=[vmem] * 5 + [smem] + [vmem] * 3 + [hbm] * 8,
        out_specs=(vmem, vmem),
        scratch_shapes=[pltpu.VMEM(a.shape, BF16) for a in held]
        + [
            pltpu.VMEM((slots, cw), BF16),
            pltpu.VMEM((tp, slots, cw), BF16),
            pltpu.VMEM((tp, slots, ff), BF16),
            pltpu.VMEM((slots, cw), BF16),
            pltpu.VMEM((slots, cw), BF16),
            pltpu.VMEM((tokens, slots), BF16),
            pltpu.VMEM((tokens, slots), BF16),
            pltpu.VMEM((block_len, width), BF16),
            pltpu.VMEM((block_len, width), BF16),
            pltpu.VMEM((block_len, width), F32),
            pltpu.VMEM((heads, dk, dk), F32),
            pltpu.VMEM((1 + rounds, heads, dk, dk), BF16),
            pltpu.VMEM((fan + rounds, heads, dk, dk), BF16),
            pltpu.VMEM((block_len, width), BF16),
            pltpu.VMEM((tp, rb, model), BF16),
            pltpu.VMEM((ys, rb, model), BF16),
            pltpu.VMEM((max(ys - 1, 1), rb, model), BF16),
            pltpu.VMEM((max(ys - 1, 1), rb, model), BF16),
            dma((8,)),
            dma((ep,)), dma((ep,)),
            dma((ys, nf)), dma((ys, nf)), dma((ys, nf)), dma((ys, nf)),
            dma((ys, nm)), dma((ys, nm)), dma((ys, nm)), dma((ys, nm)),
            dma((ep,)), dma((ep,)),
            dma((fan + rounds,)), dma((fan + rounds,)),
            dma((ys,)), dma((ys,)), dma((ys,)), dma((ys,)),
        ],
        compiler_params=pltpu.CompilerParams(
            collective_id=0, has_side_effects=True, vmem_limit_bytes=60 * 2**20
        ),
    )(
        token_rows, token_gain[None, :], route_ids, route_ids.T, route_weights,
        decay_rate, head_gain[None, :], cos_t, sin_t,
        *big,
    )


def solution(mesh):
    placed = (
        P("ep", "tp"), P("ep", "tp"), P("ep", "tp"), P("ep", "tp"),
        P("tp"), P("tp"), P("tp", None), P("ep", None), P(),
        P("ep", None), P("ep", None),
        P("ep", None, "tp"), P("ep", None, "tp"), P("ep", None, "tp"),
    )
    return jax.shard_map(
        body,
        mesh=mesh,
        in_specs=placed,
        out_specs=(P(("ep", "tp"), None), P("ep", "tp")),
        check_vma=False,
    )
```

time: 218 us -> 108 us (0.50)
  Pallas kernels: 0 us -> 96.9 us
  waiting for transfers between devices: 67.5 us -> 0 us
  blocking collectives: 49.1 us -> 0 us
  matrix products: 31.9 us -> 0 us
  other arithmetic: 22.2 us -> 1.99 us
  local copies, waits for them, and re-layouts: 25.9 us -> 6.39 us
  between operations: 14.8 us -> 0.66 us
  starting transfers between devices: 5.67 us -> 0 us
    pallas_call x0 -> x1, Pallas kernels: none -> 96.9 us  [body(): pl.pallas_call(functools.partial(kernel, size), out_shape=(jax.ShapeDtype...]
    all_gather x3 -> x0, waiting for transfers between devices: 47 us -> none  [the longest x1 29.7 us: finish(): lax.all_gather(hidden, 'tp', axis=1, tiled=True)]
    dot_general x7 -> x0, matrix products: 31.9 us -> none  [the longest x1 8.35 us: finish(): jnp.dot(lax.all_gather(hidden, 'tp', axis=1, tiled=True), down_local, pre...]
    all_to_all x1 -> x0, blocking collectives: 27.3 us -> none  [expert_part(): lax.all_to_all(outgoing, 'ep', split_axis=0, concat_axis=0, tiled=True)]
    unnamed x1 -> x0, blocking collectives: 21.8 us -> none
    all_to_all x1 -> x0, waiting for transfers between devices: 20.4 us -> none  [finish(): return lax.all_to_all(result, 'ep', split_axis=0, concat_axis=0, tiled=True)]
    select_n x11 -> x0, other arithmetic: 8.55 us -> none  [the longest x8 8.52 us: turn(): return jax.tree.map(lambda a, b: jnp.where(reached, a, b), new, before)]
    unnamed x34 -> x4, local copies, waits for them, and re-layouts: 13.4 us -> 6.39 us
  transfers between devices with their start and end apart: 5 -> 0, of which waited for: 4 -> 0; matrix products, arithmetic and copies ran while one was open for 31% -> 0% of each run, Pallas kernels for 0% -> 0%
where the time goes in v1:
time: 108 us; the launch traced here: 106 us
  Pallas kernels  96.9 us (90%)
  local copies, waits for them, and re-layouts  6.39 us (6%)
  other arithmetic  1.99 us (2%)
    pallas_call x1, Pallas kernels, body(): pl.pallas_call(functools.partial(kernel, size), out_shape=(jax.ShapeDtype...  96.9 us
    unnamed x4, local copies, waits for them, and re-layouts  6.39 us

profile of v1, /device:TPU:0, one launch (start us, length us, event | category | flops | bytes accessed | tf_op | source)
XLA Modules:
  0.0 105.9 jit_solution(6372472714793817857)
XLA Ops:
  0.7 1.0 fusion
  1.7 1.0 pad_maximum_fusion
  2.6 1.4 %copy.16.ids = s32[192,2]{1,0:T(8,128)} copy(s32[192,2]{0,1:T(2,128)} %param.23) | data formatting | bytes 3072 | tf_op args[9]
  4.1 1.5 %copy.17.rweights = f32[192,2]{1,0:T(8,128)} copy(f32[192,2]{0,1:T(2,128)} %param.24) | data formatting | bytes 3072 | tf_op args[10]
  5.5 96.9 %shard_map.149 = (bf16[128,2048]{1,0:T(8,128)(2,1)}, bf16[192,512]{1,0:T(8,128)(2,1)}) custom-call(bf16[192,2048]{1,0:T(8,128)(2,1)} %tok.1, f32[1,2048]{1,0:T(1,128)} %bitcast.9, s32[192,2]{1,0:T(8,128)} %copy.16.ids, s32[2,192]{1,0:T(2,128)} %bitcast.10, f32[192,2]{1,0:T(8,128)} %copy.17.rweights, f32[4]{0:T(128)} %decay.1, f32[1,512]{1,0:T(1,128)} %bitcast.11, ...), custom_call_target="tpu_custom_call" | custom-call | tf_op jit(solution)/shard_map/pallas_call | solution.py:414
  102.4 1.9 %copy.20 = bf16[128,2048]{1,0:T(8,128)(2,1)} copy(bf16[128,2048]{1,0:T(8,128)(2,1)} %get-tuple-element.9) | data formatting | bytes 1048576
  104.3 1.6 %copy.21 = bf16[192,512]{1,0:T(8,128)(2,1)} copy(bf16[192,512]{1,0:T(8,128)(2,1)} %get-tuple-element.10) | data formatting | bytes 393216
  (2 shorter events, 0.0 us)
